TPU v7x, 512 devices: a whole 4x8x8 slice. The times are simulated.
512 devices in a mesh: fs: 128 (over z, y, core), tp: 4 (over x).
Axes of the slice: x: 4, y: 8, z: 8, core: 2. Of those that a mesh axis runs over, the one named last changes fastest.
Arguments:
- inputs: bfloat16 [73728, 2048], P('fs'), may hold values from -24 to 24
- query_cotangent: bfloat16 [73728, 1024], P('fs', 'tp'), may hold values from -0.017944336 to 0.017944336
- value_cotangent: bfloat16 [73728, 1024], P('fs', 'tp'), may hold values from -0.017944336 to 0.017944336
- weights_query: float32 [2048, 1024], P('fs', 'tp'), may hold values from -6 to 6
- weights_value: float32 [2048, 1024], P('fs', 'tp'), may hold values from -6 to 6
- basis_query: bfloat16 [1024, 32], P('tp'), may hold values from -0.75 to 0.75
- basis_value: bfloat16 [1024, 32], P('tp'), may hold values from -0.75 to 0.75
- first_query: float32 [2048, 512], P('fs', 'tp'), may hold values from -5.4 to 5.4, as said below
- second_query: float32 [2048, 512], P('fs', 'tp'), may hold values from 0.05 to 1
- first_value: float32 [2048, 512], P('fs', 'tp'), may hold values from -5.4 to 5.4, as said below
- second_value: float32 [2048, 512], P('fs', 'tp'), may hold values from 0.05 to 1
Outputs:
- step_query: float32 [2048, 1024], P('fs', 'tp')
- step_value: float32 [2048, 1024], P('fs', 'tp')
- new_query: float32 [2048, 1024], P('fs', 'tp')
- new_value: float32 [2048, 1024], P('fs', 'tp')
- copy_query: bfloat16 [2048, 1024], P(None, 'tp')
- copy_value: bfloat16 [2048, 1024], P(None, 'tp')
- moment_query: float32 [2048, 512], P('fs', 'tp')
- square_query: float32 [2048, 512], P('fs', 'tp')
- moment_value: float32 [2048, 512], P('fs', 'tp')
- square_value: float32 [2048, 512], P('fs', 'tp')
Inputs may be any that keep to these rules, and one draw needn't show every extreme that they name: `first_query`: first moments, with a spread of scale from row to row. `first_value`: first moments, with a spread of scale from row to row.
All inputs are finite; a program needn't handle non-finite values.
Results may differ from a plain program's by a relative error of at most 0.003.
Values may be sent and summed in bfloat16 or wider, within the bound.
A program may use at most 64 MiB of HBM per device.

v0:
```python
import jax
import jax.numpy as jnp
from jax import lax
from jax.sharding import Mesh
from jax.sharding import PartitionSpec as P

D = 2048
HEADS = 16
HEAD = 64
RK = 32
FS = ("fs_0", "fs_1", "fs_2")
FS_TP = ("fs_0", "fs_1", "fs_2", "tp")


def reduced_to_own(parts, axes, order):
    dims = [lax.axis_size(a) for a in axes]
    parts = parts.reshape(*dims, *parts.shape[1:])
    parts = parts.transpose(*order, *range(len(axes), parts.ndim))
    parts = parts.reshape(-1, *parts.shape[len(axes) :])
    for k in order:
        parts = lax.psum_scatter(parts, axes[k], scatter_dimension=0, tiled=True)
    return parts[0]


def in_blocks(value, dim, size):
    dims = value.shape
    parts = value.reshape(*dims[:dim], size, dims[dim] // size, *dims[dim + 1 :])
    return jnp.moveaxis(parts, dim, 0)


def scatter_axes(value, axes, order, dim):
    size = lax.axis_size(axes)
    return reduced_to_own(in_blocks(value, dim, size), axes, order)


def one_axis_at_a_time(value, axes):
    for axis in axes:
        value = lax.psum(value, axis)
    return value


def in_one_piece(arrays, axis, dim, along):
    widths = [a.shape[along] for a in arrays]
    both = jnp.concatenate(arrays, axis=along)
    filled = lax.all_gather(both, axis, axis=dim, tiled=True)
    return tuple(jnp.split(filled, [sum(widths[:k]) for k in range(1, len(widths))], axis=along))


def from_space(direction, factor, heads_here):
    count = direction.shape[0]
    split = direction.reshape(count, heads_here, RK)
    out = jnp.einsum("nhr,hdr->nhd", split, factor, precision=lax.Precision.HIGHEST)
    return out.reshape(count, heads_here * HEAD)


def moments(reduced, first, second):
    moment = 0.9 * first + 0.1 * reduced
    square = 0.95 * second + 0.05 * reduced * reduced
    direction = moment / (jnp.sqrt(square) + 1e-08)
    return (moment, square, direction)


def per_device(
    inputs,
    query_cotangent,
    value_cotangent,
    weights_query,
    weights_value,
    basis_query,
    basis_value,
    first_query,
    second_query,
    first_value,
    second_value,
):
    own_cols = weights_query.shape[1]
    heads_here = own_cols // HEAD
    space_cols = heads_here * RK
    factor_q = basis_query.reshape(heads_here, HEAD, RK).astype(jnp.float32)
    factor_v = basis_value.reshape(heads_here, HEAD, RK).astype(jnp.float32)
    contract = (((0,), (0,)), ((), ()))
    tok_count = query_cotangent.shape[0]
    bf_q = basis_query.reshape(heads_here, HEAD, RK)
    bf_v = basis_value.reshape(heads_here, HEAD, RK)
    small_q = jnp.einsum(
        "thd,hdr->thr",
        query_cotangent.reshape(tok_count, heads_here, HEAD),
        bf_q,
        preferred_element_type=jnp.float32,
    )
    small_v = jnp.einsum(
        "thd,hdr->thr",
        value_cotangent.reshape(tok_count, heads_here, HEAD),
        bf_v,
        preferred_element_type=jnp.float32,
    )
    small_both = jnp.concatenate(
        (small_q.reshape(tok_count, space_cols), small_v.reshape(tok_count, space_cols)), axis=1
    )
    upper_part = small_both.astype(jnp.bfloat16)
    lower_part = (small_both - upper_part.astype(jnp.float32)).astype(jnp.bfloat16)
    high = lax.dot_general(inputs, upper_part, contract, preferred_element_type=jnp.float32)
    reduced = scatter_axes(
        high + lax.dot_general(inputs, lower_part, contract, preferred_element_type=jnp.float32),
        FS,
        (2, 0, 1),
        0,
    )
    reduced_q = reduced[:, :space_cols]
    reduced_v = reduced[:, space_cols:]
    moment_q, square_q, direction_q = moments(reduced_q, first_query, second_query)
    moment_v, square_v, direction_v = moments(reduced_v, first_value, second_value)
    total_q, total_v = (
        one_axis_at_a_time(jnp.sum(direction_q * direction_q), FS_TP),
        one_axis_at_a_time(jnp.sum(direction_v * direction_v), FS_TP),
    )
    entries = D * HEADS * RK
    scale_q = 1.0 / jnp.sqrt(total_q / entries + 0.25)
    scale_v = 1.0 / jnp.sqrt(total_v / entries + 0.25)
    step_q = scale_q * from_space(direction_q, factor_q, heads_here)
    step_v = scale_v * from_space(direction_v, factor_v, heads_here)
    fresh_q = weights_query - 0.1 * step_q
    fresh_v = weights_value - 0.1 * step_v
    copy_q, copy_v = in_one_piece(
        (fresh_q.astype(jnp.bfloat16), fresh_v.astype(jnp.bfloat16)), FS, 0, 1
    )
    return (
        step_q,
        step_v,
        fresh_q,
        fresh_v,
        copy_q,
        copy_v,
        moment_q,
        square_q,
        moment_v,
        square_v,
    )


def solution(mesh):
    torus = Mesh(mesh.devices.reshape(8, 8, 2, mesh.shape["tp"]), ("fs_0", "fs_1", "fs_2", "tp"))
    return jax.shard_map(
        per_device,
        mesh=torus,
        in_specs=(
            P(FS, None),
            P(FS, "tp"),
            P(FS, "tp"),
            P(FS, "tp"),
            P(FS, "tp"),
            P("tp", None),
            P("tp", None),
            P(FS, "tp"),
            P(FS, "tp"),
            P(FS, "tp"),
            P(FS, "tp"),
        ),
        out_specs=(
            P(FS, "tp"),
            P(FS, "tp"),
            P(FS, "tp"),
            P(FS, "tp"),
            P(None, "tp"),
            P(None, "tp"),
            P(FS, "tp"),
            P(FS, "tp"),
            P(FS, "tp"),
            P(FS, "tp"),
        ),
        check_vma=False,
    )
```

profile of v0, /device:TPU:1, one launch (start us, length us, event | category | flops | bytes accessed | tf_op | source)
XLA Modules:
  0.0 274.1 jit_solution(18366344088311440782)
XLA Ops:
  7.2 0.0 reduce-scatter.4.cloned.1.call-start
  7.2 1.0 reshape.55
  8.2 0.8 reshape.58
  9.0 1.2 copy.41
  10.2 1.2 copy.43
  11.3 0.2 fusion.12
  11.5 0.2 fusion.9
  11.7 1.0 fusion.4
  12.7 2.3 fusion
  15.1 2.9 %copy.45 = f32[2048,256]{1,0:T(8,128)} copy(f32[2048,256]{0,1:T(8,128)} %fusion) | data formatting | bytes 4194304 | tf_op jit(solution)/shard_map/add | solution.py:104
  18.0 3.1 %copy.46 = f32[2,8,8,16,256]{4,3,2,1,0:T(8,128)} copy(f32[2,8,8,16,256]{4,3,0,2,1:T(8,128)} %bitcast.28) | data formatting | bytes 4194304 | tf_op jit(solution)/shard_map/transpose | solution.py:18
  21.2 0.0 reduce-scatter.6.cloned.1.call-start
  21.2 24.5 %reduce-scatter.4.cloned.1.call-done = f32[64,16,256]{2,1,0:T(8,128)} async-done(((f32[128,16,256]{2,1,0:T(8,128)}), f32[64,16,256]{2,1,0:T(8,128)}) %reduce-scatter.4.cloned.1.call-update) | async-done | bytes 1048592 | tf_op jit(solution)/shard_map/reduce_scatter | solution.py:21
  45.7 0.0 reduce-scatter.8.cloned.1.call-start
  45.8 41.3 %reduce-scatter.6.cloned.1.call-done = f32[8,16,256]{2,1,0:T(8,128)} async-done(((f32[64,16,256]{2,1,0:T(8,128)}), f32[8,16,256]{2,1,0:T(8,128)}) %reduce-scatter.6.cloned.1.call-update) | async-done | bytes 131088 | tf_op jit(solution)/shard_map/reduce_scatter | solution.py:21
  87.0 0.0 all-gather.2.cloned.1.call-start
  87.1 39.1 %reduce-scatter.8.cloned.1.call-done = f32[1,16,256]{2,1,0:T(8,128)} async-done(((f32[8,16,256]{2,1,0:T(8,128)}), f32[1,16,256]{2,1,0:T(8,128)}) %reduce-scatter.8.cloned.1.call-update) | async-done | bytes 16400 | tf_op jit(solution)/shard_map/reduce_scatter | solution.py:21
  126.2 1.9 multiply_reduce_fusion
  128.1 15.0 %all-reduce.1 = (f32[]{:T(128)}, f32[]{:T(128)}) all-reduce(f32[]{:T(128)} %get-tuple-element.32, f32[]{:T(128)} %get-tuple-element.22), channel_id=1, replica_groups=mesh['fs_0'=8,'fs_1'=8,'fs_2'=2,'tp'=4] {'fs_0'}, use_global_device_ids=true, to_apply=%region_4.0 | all-reduce | flops 2 | bytes 16 | tf_op jit(solution)/shard_map/psum | solution.py:38
  143.1 12.8 %all-reduce = (f32[]{:T(128)}, f32[]{:T(128)}) all-reduce(f32[]{:T(128)} %get-tuple-element.12, f32[]{:T(128)} %get-tuple-element.13), channel_id=1, replica_groups=mesh['fs_0'=8,'fs_1'=8,'fs_2'=2,'tp'=4] {'fs_1'}, use_global_device_ids=true, to_apply=%region_5.0 | all-reduce | flops 2 | bytes 16 | tf_op jit(solution)/shard_map/psum | solution.py:38
  155.9 16.1 %all-reduce.3 = (f32[]{:T(128)}, f32[]{:T(128)}) all-reduce(f32[]{:T(128)} %get-tuple-element.10, f32[]{:T(128)} %get-tuple-element.11), channel_id=1, replica_groups=mesh['fs_0'=8,'fs_1'=8,'fs_2'=2,'tp'=4] {'fs_2'}, use_global_device_ids=true, to_apply=%region_6.0 | all-reduce | flops 2 | bytes 16 | tf_op jit(solution)/shard_map/psum | solution.py:38
  172.0 9.0 %all-reduce.2 = (f32[]{:T(128)}, f32[]{:T(128)}) all-reduce(f32[]{:T(128)} %get-tuple-element.16, f32[]{:T(128)} %get-tuple-element.17), channel_id=1, replica_groups=mesh['fs_0'=8,'fs_1'=8,'fs_2'=2,'tp'=4] {'tp'}, use_global_device_ids=true, to_apply=%region_7.0 | all-reduce | flops 2 | bytes 16 | tf_op jit(solution)/shard_map/psum | solution.py:38
  182.4 0.1 reshape.63
  182.4 0.1 fusion.1
  182.6 0.1 mul.85
  182.7 0.1 reshape.62
  182.8 0.1 fusion.2
  183.0 0.1 mul.75
  183.1 0.6 fusion.18
  183.7 0.6 pad_maximum_fusion.1
  184.3 80.3 %all-gather.2.cloned.1.call-done = bf16[2048,512]{1,0:T(8,128)(2,1)} async-done(((bf16[16,512]{1,0:T(8,128)(2,1)}), bf16[2048,512]{1,0:T(8,128)(2,1)}) %all-gather.2.cloned.1.call-update) | async-done | bytes 2097168 | tf_op jit(solution)/shard_map/all_gather | solution.py:45
  264.6 3.0 %fusion.22 = (bf16[2048,256]{1,0:T(8,128)(2,1)}, bf16[2048,256]{1,0:T(8,128)(2,1)}) fusion(bf16[2048,512]{1,0:T(8,128)(2,1)} %all-gather.2.cloned.1.call-done), kind=kLoop, calls=%fused_computation.35 | loop fusion | bytes 4194304 | tf_op jit(solution)/shard_map/split | solution.py:46
  (24 shorter events, 0.1 us)
Async XLA Ops:
  7.2 4.6 %copy-start = (bf16[576,2048]{1,0:T(8,128)(2,1)S(1)}, bf16[576,2048]{1,0:T(8,128)(2,1)}, u32[]{:S(2)}) copy-start(bf16[576,2048]{1,0:T(8,128)(2,1)} %param.11) | copy-start | bytes 7077892
  7.2 38.5 %reduce-scatter.4.cloned.1.call-start = ((), (), s32[]{:S(2)}) async-start(), calls=%async_computation.3 | async-start | bytes 3145728 | tf_op jit(solution)/shard_map/reduce_scatter | solution.py:21
  21.1 105.0 %copy-start.5 = (f32[16,128]{1,0:T(8,128)S(1)}, f32[16,128]{1,0:T(8,128)}, u32[]{:S(2)}) copy-start(f32[16,128]{1,0:T(8,128)} %param.21) | copy-start | bytes 24580
  21.1 105.0 %copy-start.6 = (f32[16,128]{1,0:T(8,128)S(1)}, f32[16,128]{1,0:T(8,128)}, u32[]{:S(2)}) copy-start(f32[16,128]{1,0:T(8,128)} %param.20) | copy-start | bytes 24580
  21.1 105.0 %copy-start.7 = (f32[16,128]{1,0:T(8,128)S(1)}, f32[16,128]{1,0:T(8,128)}, u32[]{:S(2)}) copy-start(f32[16,128]{1,0:T(8,128)} %param.19) | copy-start | bytes 24580
  21.1 105.0 %copy-start.8 = (f32[16,128]{1,0:T(8,128)S(1)}, f32[16,128]{1,0:T(8,128)}, u32[]{:S(2)}) copy-start(f32[16,128]{1,0:T(8,128)} %param.18) | copy-start | bytes 24580
  21.1 161.9 %copy-start.3 = (f32[16,256]{1,0:T(8,128)S(1)}, f32[16,256]{1,0:T(8,128)}, u32[]{:S(2)}) copy-start(f32[16,256]{1,0:T(8,128)} %param.14) | copy-start | bytes 49156
  21.1 161.9 %copy-start.4 = (f32[16,256]{1,0:T(8,128)S(1)}, f32[16,256]{1,0:T(8,128)}, u32[]{:S(2)}) copy-start(f32[16,256]{1,0:T(8,128)} %param.15) | copy-start | bytes 49156
  21.2 65.8 %reduce-scatter.6.cloned.1.call-start = ((), (), s32[]{:S(2)}) async-start(), calls=%async_computation.4 | async-start | bytes 1179648 | tf_op jit(solution)/shard_map/reduce_scatter | solution.py:21
  45.7 80.5 %reduce-scatter.8.cloned.1.call-start = ((), (), s32[]{:S(2)}) async-start(), calls=%async_computation.5 | async-start | bytes 147456 | tf_op jit(solution)/shard_map/reduce_scatter | solution.py:21
  87.0 177.6 %all-gather.2.cloned.1.call-start = ((), (), s32[]{:S(2)}) async-start(), calls=%async_computation.6 | async-start | bytes 2113536 | tf_op jit(solution)/shard_map/all_gather | solution.py:45
  182.7 84.9 %copy-start.1 = (f32[16,256]{1,0:T(8,128)}, f32[16,256]{1,0:T(8,128)S(1)}, u32[]{:S(2)}) copy-start(f32[16,256]{1,0:T(8,128)S(1)} %mul.85) | copy-start | bytes 49156
  183.1 84.5 %copy-start.2 = (f32[16,256]{1,0:T(8,128)}, f32[16,256]{1,0:T(8,128)S(1)}, u32[]{:S(2)}) copy-start(f32[16,256]{1,0:T(8,128)S(1)} %mul.75) | copy-start | bytes 49156
Sparse Core Ops, SparseCore 0:
  21.3 24.3 reduce-scatter.3
  48.5 38.4 reduce-scatter.5
  89.8 36.3 reduce-scatter.7
  184.4 80.1 all-gather.1
where the time goes:
time: 275 us; the launch traced here: 274 us
  waiting for transfers between devices  185 us (67%)
  blocking collectives  52.9 us (19%)
  between operations  15.3 us (6%)
  local copies, waits for them, and re-layouts  13.6 us (5%)
  matrix products  3.98 us (1%)
  other arithmetic  3.17 us (1%)
    reduce_scatter x3, waiting for transfers between devices, reduced_to_own(): parts = lax.psum_scatter(parts, axes[k], scatter_dimension=0, tiled=True)  105 us
    all_gather x1, waiting for transfers between devices, in_one_piece(): filled = lax.all_gather(both, axis, axis=dim, tiled=True)  80.3 us
    psum x4, blocking collectives, one_axis_at_a_time(): value = lax.psum(value, axis)  52.9 us
  transfers between devices with their start and end apart: 4, of which 4 were waited for; matrix products, arithmetic and copies ran while one was open for 0% of the time, Pallas kernels for 0%

commit v1 on v0

v1 whole, which is shorter than its diff:
```python
import functools

import jax
import jax.numpy as jnp
from jax import lax
from jax.experimental import pallas as pl
from jax.experimental.pallas import tpu as pltpu
from jax.sharding import PartitionSpec as P

D = 2048
HEADS = 16
HEAD = 64
RK = 32
N = 8
ORDER = (4, 3, 5, 2, 6, 1, 7)
BF = jnp.bfloat16
F32 = jnp.float32
MESH = pl.DeviceIdType.MESH
ANY = pl.BlockSpec(memory_space=pl.ANY)
VM = pl.BlockSpec(memory_space=pltpu.VMEM)


def spread(basis):
    rows, rank = basis.shape
    heads = rows // HEAD
    wide = heads * rank
    copies = lax.broadcasted_iota(jnp.int32, (rank, wide), 1) % rank
    pick = (lax.broadcasted_iota(jnp.int32, (rank, wide), 0) == copies).astype(BF)
    tiled = jnp.dot(basis, pick, preferred_element_type=F32)
    row = lax.broadcasted_iota(jnp.int32, (rows, wide), 0) // HEAD
    col = lax.broadcasted_iota(jnp.int32, (rows, wide), 1) // rank
    return jnp.where(row == col, tiled, 0.0).astype(BF)


def moments(reduced, first, second):
    moment = 0.9 * first + 0.1 * reduced
    square = 0.95 * second + 0.05 * reduced * reduced
    direction = moment / (jnp.sqrt(square) + 1e-08)
    return moment, square, direction


def encode(w):
    s = w * w
    return jnp.where(w < 0, -(s * s), s * s).astype(BF)


def decode(code):
    c = code.astype(F32)
    size = lax.rsqrt(lax.rsqrt(jnp.maximum(jnp.abs(c), 1e-30)))
    return jnp.where(c < 0, -size, size)


def talk(
    x_hbm, qc_hbm, vc_hbm, bq_hbm, bv_hbm, wq_hbm, wv_hbm, fq_hbm, sq_hbm, fv_hbm, sv_hbm,
    dq_out, dv_out, wq_out, wv_out, red_out, ss_out,
    x, qc, vc, bq, bv, wq, wv, mom, small, mine, d2d_send, d2d_recv,
    send_q, recv_q, send_v, recv_v, send2_q, recv2_q, send2_v, recv2_v,
    dq, dv, wall_q, wall_v, red, ss, load_sem, ssem, rsem,
):
    fs = lax.axis_index("fs")
    tp = lax.axis_index("tp")
    c = fs % 2
    y = (fs // 2) % N
    z = fs // (2 * N)
    other = fs + 1 - 2 * c

    def on_y(k):
        return {"fs": (z * N + (y + k) % N) * 2 + c}

    def on_z(k):
        return {"fs": (((z + k) % N) * N + y) * 2 + c}

    partner = {"fs": other}
    over_x = [{"fs": f, "tp": (tp + k) % 4} for f, k in
              [(fs, 1), (fs, 2), (fs, 3), (other, 0), (other, 1), (other, 2), (other, 3)]]

    barrier = pltpu.get_barrier_semaphore()
    greeted = [on_y(k) for k in ORDER] + [on_z(k) for k in ORDER] + over_x
    for device in greeted:
        pl.semaphore_signal(barrier, inc=1, device_id=device, device_id_type=MESH)

    loads = []

    def load(src, dst):
        copy = pltpu.make_async_copy(src, dst, load_sem.at[len(loads)])
        copy.start()
        loads.append(copy)
        return copy

    sent = []

    def send(src, dst, device):
        at = len(sent)
        copy = pltpu.make_async_remote_copy(
            src_ref=src, dst_ref=dst, send_sem=ssem.at[at], recv_sem=rsem.at[at],
            device_id=device, device_id_type=MESH)
        copy.start()
        sent.append(copy)
        return copy

    first = [load(bq_hbm, bq), load(bv_hbm, bv), load(qc_hbm, qc), load(vc_hbm, vc)]
    order = ORDER + (0,)
    chunk_z = [(z + k) % N for k in order]
    chunks = [
        load(x_hbm.at[:, pl.ds(pl.multiple_of(chunk_z[j] * 256, 256), 256)], x.at[j]) for j in range(N)
    ]
    later_w = [load(wq_hbm, wq), load(wv_hbm, wv)]
    later_m = [load(r, mom.at[i]) for i, r in enumerate((fq_hbm, sq_hbm, fv_hbm, sv_hbm))]

    for copy in first:
        copy.wait()
    small[:, :128] = jnp.dot(qc[...], spread(bq[...]), preferred_element_type=F32).astype(BF)
    small[:, 128:] = jnp.dot(vc[...], spread(bv[...]), preferred_element_type=F32).astype(BF)

    d2d = []

    def product(j):
        chunks[j].wait()
        out = lax.dot_general(x[j], small[...], (((0,), (0,)), ((), ())), preferred_element_type=F32)
        out = out.reshape(N, 2, 16, 256)
        p0, p1 = out[:, 0], out[:, 1]
        own = jnp.where(c == 0, p0, p1)
        away = jnp.where(c == 0, p1, p0).astype(BF)
        mine[j, 0] = own[:, :, :128]
        mine[j, 1] = own[:, :, 128:]
        d2d_send[j, 0] = away[:, :, :128]
        d2d_send[j, 1] = away[:, :, 128:]

    rs1_v = []

    def combine(j):
        d2d[j].wait_recv()
        send_q[:, pl.ds(chunk_z[j], 1)] = (mine[j, 0] + d2d_recv[j, 0].astype(F32)).astype(BF)[:, None]
        send_v[j] = (mine[j, 1] + d2d_recv[j, 1].astype(F32)).astype(BF)
        if order[j] != 0:
            rs1_v.append((order[j], send(send_v.at[j], recv_v.at[order[j]], on_z(order[j]))))

    product(0)
    pl.semaphore_wait(barrier, len(greeted))

    for copy in later_w:
        copy.wait()
    wall_q[pl.ds(c, 1), pl.ds(y, 1), pl.ds(z, 1)] = encode(wq[...])[None, None, None]
    wall_v[pl.ds(c, 1), pl.ds(z, 1), pl.ds(y, 1)] = encode(wv[...])[None, None, None]
    d2d.append(send(d2d_send.at[0], d2d_recv.at[0], partner))
    w1 = []
    for k in ORDER:
        w1.append(send(wall_q.at[c, y, z], wall_q.at[c, y, z], on_z(k)))
        w1.append(send(wall_v.at[c, z, y], wall_v.at[c, z, y], on_y(k)))
    for j in range(1, N):
        product(j)
        d2d.append(send(d2d_send.at[j], d2d_recv.at[j], partner))
        combine(j - 1)
    combine(N - 1)
    rs1_q = [(k, send(send_q.at[(y + k) % N], recv_q.at[k], on_y(k))) for k in ORDER]

    forwards = []

    def forward(ref, index):
        forwards.append(send(ref.at[c, index], ref.at[c, index], partner))

    for copy in w1:
        copy.wait_recv()
    right, left = [], []

    def w_step(s):
        if s > 0:
            right[-2].wait_recv()
            right[-1].wait_recv()
            forward(wall_q, (y + N - s) % N)
            forward(wall_v, (z + N - s) % N)
            if s < 4:
                left[-2].wait_recv()
                left[-1].wait_recv()
                forward(wall_q, (y + s) % N)
                forward(wall_v, (z + s) % N)
        else:
            forward(wall_q, y)
            forward(wall_v, z)
        if s < 4:
            a, b = (y + N - s) % N, (z + N - s) % N
            right.append(send(wall_q.at[c, a], wall_q.at[c, a], on_y(1)))
            right.append(send(wall_v.at[c, b], wall_v.at[c, b], on_z(1)))
        if s < 3:
            a, b = (y + s) % N, (z + s) % N
            left.append(send(wall_q.at[c, a], wall_q.at[c, a], on_y(N - 1)))
            left.append(send(wall_v.at[c, b], wall_v.at[c, b], on_z(N - 1)))

    w_step(0)

    total_v = send_v[N - 1].astype(F32)
    for k, copy in rs1_v:
        copy.wait_recv()
        total_v = total_v + recv_v[k].astype(F32)
    send2_v[...] = total_v.astype(BF)
    rs2_v = [(k, send(send2_v.at[(y + k) % N], recv2_v.at[k], on_y(k))) for k in ORDER]
    total_q = send_q[pl.ds(y, 1)][0].astype(F32)
    for k, copy in rs1_q:
        copy.wait_recv()
        total_q = total_q + recv_q[k].astype(F32)
    send2_q[...] = total_q.astype(BF)
    rs2_q = [(k, send(send2_q.at[(z + k) % N], recv2_q.at[k], on_z(k))) for k in ORDER]
    w_step(1)

    reduced_v = send2_v[pl.ds(y, 1)][0].astype(F32)
    for k, copy in rs2_v:
        copy.wait_recv()
        reduced_v = reduced_v + recv2_v[k].astype(F32)
    reduced_q = send2_q[pl.ds(z, 1)][0].astype(F32)
    for k, copy in rs2_q:
        copy.wait_recv()
        reduced_q = reduced_q + recv2_q[k].astype(F32)
    for copy in later_m:
        copy.wait()
    red[0] = reduced_q
    red[1] = reduced_v
    direction_q = moments(reduced_q, mom[0], mom[1])[2]
    direction_v = moments(reduced_v, mom[2], mom[3])[2]
    dq[pl.ds(c, 1), pl.ds(y, 1), pl.ds(z, 1)] = direction_q.astype(BF)[None, None, None]
    dv[pl.ds(c, 1), pl.ds(z, 1), pl.ds(y, 1)] = direction_v.astype(BF)[None, None, None]
    ag1 = []
    for k in ORDER:
        ag1.append(send(dq.at[c, y, z], dq.at[c, y, z], on_z(k)))
        ag1.append(send(dv.at[c, z, y], dv.at[c, z, y], on_y(k)))
    w_step(2)
    for copy in ag1:
        copy.wait_recv()
    ag2 = []
    for k in ORDER:
        ag2.append((k, send(dq.at[c, y], dq.at[c, y], on_y(k)), send(dv.at[c, z], dv.at[c, z], on_z(k))))
    forward(dq, y)
    forward(dv, z)
    w_step(3)

    def squares(ref, index):
        t = ref[pl.ds(c, 1), pl.ds(index, 1)].astype(F32).reshape(N * 2, 8, 128)
        return jnp.sum(t * t, axis=0)

    ss_q = squares(dq, y)
    ss_v = squares(dv, z)
    for k, copy_q, copy_v in sorted(ag2, key=lambda t: min(t[0], N - t[0])):
        a, b = (y + N - k) % N, (z + N - k) % N
        copy_q.wait_recv()
        forward(dq, a)
        ss_q = ss_q + squares(dq, a)
        copy_v.wait_recv()
        forward(dv, b)
        ss_v = ss_v + squares(dv, b)
    ss[0, 0] = ss_q
    ss[0, 1] = ss_v
    sums = [send(ss.at[0], ss.at[1 + i], device) for i, device in enumerate(over_x)]
    w_step(4)
    for copy in forwards:
        copy.wait_recv()
    at = len(loads)
    outs = [load(dq, dq_out), load(dv, dv_out), load(wall_q, wq_out), load(wall_v, wv_out), load(red, red_out)]
    for copy in sums:
        copy.wait_recv()
    outs.append(load(ss, ss_out))
    for copy in sent:
        copy.wait_send()
    for copy in outs:
        copy.wait()


def finish(
    dq, dv, wall_q, wall_v, red, ss, bq, bv, wq, wv, fq, sq, fv, sv,
    step_q, step_v, new_q, new_v, copy_q, copy_v, moment_q, square_q, moment_v, square_v,
):
    entries = D * HEADS * RK
    sums = jnp.sum(ss[...], axis=0)
    turn = (((1,), (1,)), ((), ()))
    for which, (d, wall, b, w, f, s, step, new, copy, moment, square) in enumerate((
        (dq, wall_q, bq, wq, fq, sq, step_q, new_q, copy_q, moment_q, square_q),
        (dv, wall_v, bv, wv, fv, sv, step_v, new_v, copy_v, moment_v, square_v),
    )):
        factor = spread(b[...])
        mean = jnp.sum(jnp.sum(sums[which], axis=0, keepdims=True), axis=1, keepdims=True) / entries
        scale = 1.0 / jnp.sqrt(mean + 0.25)
        m, sqr, direction = moments(red[which], f[...], s[...])
        moment[...] = m
        square[...] = sqr
        high = direction.astype(BF)
        low = (direction - high.astype(F32)).astype(BF)
        own = lax.dot_general(high, factor, turn, preferred_element_type=F32)
        own = scale * (own + lax.dot_general(low, factor, turn, preferred_element_type=F32))
        step[...] = own
        new[...] = w[...] - 0.1 * own
        for z in range(N):
            if which == 0:
                rows, codes = d[:, :, z], wall[:, :, z]
            else:
                rows, codes = d[:, z], wall[:, z]
            rows = jnp.stack([rows[0], rows[1]], axis=1).reshape(2 * N * 16, 128)
            codes = jnp.stack([codes[0], codes[1]], axis=1).reshape(2 * N * 16, 256)
            there = lax.dot_general(rows, factor, turn, preferred_element_type=F32)
            copy[z * 256:(z + 1) * 256, :] = (decode(codes) - 0.1 * (scale * there)).astype(BF)


def per_device(x, qc, vc, wq, wv, bq, bv, fq, sq, fv, sv):
    tokens = x.shape[0]
    n_load, n_send = 32, 180
    vmem = pltpu.VMEM
    small_shape = jax.ShapeDtypeStruct
    dq, dv, wall_q, wall_v, red, ss = pl.pallas_call(
        talk,
        out_shape=(
            small_shape((2, N, N, 16, 128), BF), small_shape((2, N, N, 16, 128), BF),
            small_shape((2, N, N, 16, 256), BF), small_shape((2, N, N, 16, 256), BF),
            small_shape((2, 16, 128), F32), small_shape((8, 2, 8, 128), F32),
        ),
        in_specs=[ANY] * 11,
        out_specs=[ANY] * 6,
        scratch_shapes=[
            vmem((N, tokens, 256), BF), vmem((tokens, 256), BF), vmem((tokens, 256), BF),
            vmem((256, RK), BF), vmem((256, RK), BF), vmem((16, 256), F32), vmem((16, 256), F32),
            vmem((4, 16, 128), F32), vmem((tokens, 256), BF),
            vmem((N, 2, N, 16, 128), F32), vmem((N, 2, N, 16, 128), BF), vmem((N, 2, N, 16, 128), BF),
            vmem((N, N, 16, 128), BF), vmem((N, N, 16, 128), BF),
            vmem((N, N, 16, 128), BF), vmem((N, N, 16, 128), BF),
            vmem((N, 16, 128), BF), vmem((N, 16, 128), BF), vmem((N, 16, 128), BF), vmem((N, 16, 128), BF),
            vmem((2, N, N, 16, 128), BF), vmem((2, N, N, 16, 128), BF),
            vmem((2, N, N, 16, 256), BF), vmem((2, N, N, 16, 256), BF),
            vmem((2, 16, 128), F32), vmem((8, 2, 8, 128), F32),
            pltpu.SemaphoreType.DMA((n_load,)), pltpu.SemaphoreType.DMA((n_send,)),
            pltpu.SemaphoreType.DMA((n_send,)),
        ],
        compiler_params=pltpu.CompilerParams(collective_id=0, has_side_effects=True),
    )(x, qc, vc, bq, bv, wq, wv, fq, sq, fv, sv)
    wide, narrow = small_shape((16, 256), F32), small_shape((16, 128), F32)
    whole = small_shape((D, 256), BF)
    return pl.pallas_call(
        finish,
        out_shape=(wide, wide, wide, wide, whole, whole, narrow, narrow, narrow, narrow),
        in_specs=[VM] * 14,
        out_specs=[VM] * 10,
    )(dq, dv, wall_q, wall_v, red, ss, bq, bv, wq, wv, fq, sq, fv, sv)


def solution(mesh):
    return jax.shard_map(
        per_device,
        mesh=mesh,
        in_specs=(
            P("fs", None), P("fs", "tp"), P("fs", "tp"), P("fs", "tp"), P("fs", "tp"),
            P("tp", None), P("tp", None), P("fs", "tp"), P("fs", "tp"), P("fs", "tp"), P("fs", "tp"),
        ),
        out_specs=(
            P("fs", "tp"), P("fs", "tp"), P("fs", "tp"), P("fs", "tp"), P(None, "tp"), P(None, "tp"),
            P("fs", "tp"), P("fs", "tp"), P("fs", "tp"), P("fs", "tp"),
        ),
        check_vma=False,
    )
```

time: 275 us -> 62.3 us (0.23)
  waiting for transfers between devices: 185 us -> 0 us
  Pallas kernels: 0 us -> 58.5 us
  blocking collectives: 52.9 us -> 0 us
  between operations: 15.3 us -> 0.65 us
  local copies, waits for them, and re-layouts: 13.6 us -> 2.9 us
  matrix products: 3.98 us -> 0 us
  other arithmetic: 3.17 us -> 0 us
    reduce_scatter x3 -> x0, waiting for transfers between devices: 105 us -> none  [reduced_to_own(): parts = lax.psum_scatter(parts, axes[k], scatter_dimension=0, tiled=True)]
    all_gather x1 -> x0, waiting for transfers between devices: 80.3 us -> none  [in_one_piece(): filled = lax.all_gather(both, axis, axis=dim, tiled=True)]
    pallas_call x0 -> x2, Pallas kernels: none -> 58.5 us  [the longest x1 53.6 us: per_device(): pl.pallas_call(talk, out_shape=(small_shape((2, N, N, 16, 128), BF), smal...]
    psum x4 -> x0, blocking collectives: 52.9 us -> none  [one_axis_at_a_time(): value = lax.psum(value, axis)]
    dot_general x6 -> x0, matrix products: 3.98 us -> none  [the longest x1 2.31 us: per_device(): lax.dot_general(inputs, lower_part, contract, preferred_element_type=jnp....]
    transpose x1 -> x0, local copies, waits for them, and re-layouts: 3.13 us -> none  [reduced_to_own(): parts = parts.transpose(*order, *range(len(axes), parts.ndim))]
    split x1 -> x0, local copies, waits for them, and re-layouts: 2.99 us -> none  [in_one_piece(): jnp.split(filled, [sum(widths[:k]) for k in range(1, len(widths))], axis=...]
    add x1 -> x0, local copies, waits for them, and re-layouts: 2.93 us -> none  [per_device(): high + lax.dot_general(inputs, lower_part, contract, preferred_element_ty...]
  transfers between devices with their start and end apart: 4 -> 0, of which waited for: 4 -> 0; matrix products, arithmetic and copies ran while one was open for 0% -> 0% of each run, Pallas kernels for 0% -> 0%
where the time goes in v1:
time: 62.3 us; the launch traced here: 62.1 us
  Pallas kernels  58.5 us (94%)
  local copies, waits for them, and re-layouts  2.9 us (5%)
  between operations  0.65 us (1%)
    pallas_call x1, Pallas kernels, per_device(): pl.pallas_call(talk, out_shape=(small_shape((2, N, N, 16, 128), BF), smal...  53.6 us
    pallas_call x1, Pallas kernels, per_device(): pl.pallas_call(finish, out_shape=(wide, wide, wide, wide, whole, whole, n...  4.9 us
    unnamed x2, local copies, waits for them, and re-layouts  2.9 us

profile of v1, /device:TPU:1, one launch (start us, length us, event | category | flops | bytes accessed | tf_op | source)
XLA Modules:
  0.0 62.1 jit_solution(1704791622071397477)
XLA Ops:
  0.6 1.4 %copy.21.bq_hbm.bq = bf16[256,32]{1,0:T(8,128)(2,1)} copy(bf16[256,32]{0,1:T(8,128)(2,1)} %param.16) | data formatting | bytes 32768 | tf_op args[5]
  2.1 1.4 %copy.22.bv_hbm.bv = bf16[256,32]{1,0:T(8,128)(2,1)} copy(bf16[256,32]{0,1:T(8,128)(2,1)} %param.17) | data formatting | bytes 32768 | tf_op args[6]
  3.5 53.6 %shard_map.186 = (bf16[2,8,8,16,128]{4,3,2,1,0:T(8,128)(2,1)}, bf16[2,8,8,16,128]{4,3,2,1,0:T(8,128)(2,1)}, bf16[2,8,8,16,256]{4,3,2,1,0:T(8,128)(2,1)}, bf16[2,...) custom-call(bf16[576,2048]{1,0:T(8,128)(2,1)} %x_hbm.1, bf16[576,256]{1,0:T(8,128)(2,1)} %qc_hbm.1, ...), custom_call_target="tpu_custom_call" | custom-call | tf_op jit(solution)/shard_map/pallas_call | solution.py:305
  57.2 4.9 %shard_map.187 = (f32[16,256]{1,0:T(8,128)}, f32[16,256]{1,0:T(8,128)}, f32[16,256]{1,0:T(8,128)}, f32[16,256]{1,0:T(8,128)}, bf16[2048,256]{1,0:T(8,128)(2,1)},...) custom-call(bf16[2,8,8,16,128]{4,3,2,1,0:T(8,128)(2,1)} %get-tuple-e, ...), custom_call_target="tpu_custom_call" | custom-call | tf_op jit(solution)/shard_map/pallas_call | solution.py:332

commit v2 on v1

--- a/solution.py
+++ b/solution.py
@@ -12,23 +12,24 @@
 HEAD = 64
 RK = 32
 N = 8
+READY = 2
 ORDER = (4, 3, 5, 2, 6, 1, 7)
 BF = jnp.bfloat16
 F32 = jnp.float32
 MESH = pl.DeviceIdType.MESH
+TURN = (((1,), (1,)), ((), ()))
 ANY = pl.BlockSpec(memory_space=pl.ANY)
 VM = pl.BlockSpec(memory_space=pltpu.VMEM)
 
 
 def spread(basis):
-    rows, rank = basis.shape
-    heads = rows // HEAD
-    wide = heads * rank
-    copies = lax.broadcasted_iota(jnp.int32, (rank, wide), 1) % rank
-    pick = (lax.broadcasted_iota(jnp.int32, (rank, wide), 0) == copies).astype(BF)
-    tiled = jnp.dot(basis, pick, preferred_element_type=F32)
-    row = lax.broadcasted_iota(jnp.int32, (rows, wide), 0) // HEAD
-    col = lax.broadcasted_iota(jnp.int32, (rows, wide), 1) // rank
+    rank, rows = basis.shape
+    wide = rows // HEAD * rank
+    copies = lax.broadcasted_iota(jnp.int32, (wide, rank), 0) % rank
+    pick = (lax.broadcasted_iota(jnp.int32, (wide, rank), 1) == copies).astype(BF)
+    tiled = jnp.dot(pick, basis, preferred_element_type=F32)
+    row = lax.broadcasted_iota(jnp.int32, (wide, rows), 0) // rank
+    col = lax.broadcasted_iota(jnp.int32, (wide, rows), 1) // HEAD
     return jnp.where(row == col, tiled, 0.0).astype(BF)
 
 
@@ -53,7 +54,7 @@
 def talk(
     x_hbm, qc_hbm, vc_hbm, bq_hbm, bv_hbm, wq_hbm, wv_hbm, fq_hbm, sq_hbm, fv_hbm, sv_hbm,
     dq_out, dv_out, wq_out, wv_out, red_out, ss_out,
-    x, qc, vc, bq, bv, wq, wv, mom, small, mine, d2d_send, d2d_recv,
+    x, qc, vc, bq, bv, wq, wv, mom, small, parts, d2d_recv,
     send_q, recv_q, send_v, recv_v, send2_q, recv2_q, send2_v, recv2_v,
     dq, dv, wall_q, wall_v, red, ss, load_sem, ssem, rsem,
 ):
@@ -109,50 +110,58 @@
 
     for copy in first:
         copy.wait()
-    small[:, :128] = jnp.dot(qc[...], spread(bq[...]), preferred_element_type=F32).astype(BF)
-    small[:, 128:] = jnp.dot(vc[...], spread(bv[...]), preferred_element_type=F32).astype(BF)
+    small[:128] = lax.dot_general(spread(bq[...]), qc[...], TURN, preferred_element_type=F32).astype(BF)
+    small[128:] = lax.dot_general(spread(bv[...]), vc[...], TURN, preferred_element_type=F32).astype(BF)
 
     d2d = []
 
     def product(j):
         chunks[j].wait()
-        out = lax.dot_general(x[j], small[...], (((0,), (0,)), ((), ())), preferred_element_type=F32)
-        out = out.reshape(N, 2, 16, 256)
-        p0, p1 = out[:, 0], out[:, 1]
-        own = jnp.where(c == 0, p0, p1)
-        away = jnp.where(c == 0, p1, p0).astype(BF)
-        mine[j, 0] = own[:, :, :128]
-        mine[j, 1] = own[:, :, 128:]
-        d2d_send[j, 0] = away[:, :, :128]
-        d2d_send[j, 1] = away[:, :, 128:]
+        out = jnp.dot(small[...], x[j], preferred_element_type=F32).astype(BF).T.reshape(N, 2, 16, 256)
+        for core in range(2):
+            parts[j, core, 0] = out[:, core, :, :128]
+            parts[j, core, 1] = out[:, core, :, 128:]
+        if j >= READY:
+            give(j)
+
+    def give(j):
+        d2d.append(send(parts.at[j, 1 - c], d2d_recv.at[j], partner))
 
     rs1_v = []
+
+    rs1_q = []
 
     def combine(j):
         d2d[j].wait_recv()
-        send_q[:, pl.ds(chunk_z[j], 1)] = (mine[j, 0] + d2d_recv[j, 0].astype(F32)).astype(BF)[:, None]
-        send_v[j] = (mine[j, 1] + d2d_recv[j, 1].astype(F32)).astype(BF)
+        both = (parts[j, pl.ds(c, 1)][0].astype(F32) + d2d_recv[j].astype(F32)).astype(BF)
+        send_q[:, j] = both[0]
+        send_v[j] = both[1]
         if order[j] != 0:
             rs1_v.append((order[j], send(send_v.at[j], recv_v.at[order[j]], on_z(order[j]))))
-
-    product(0)
+        if j % 2:
+            for k in ORDER:
+                span = pl.ds(j - 1, 2)
+                rs1_q.append((k, j // 2, send(send_q.at[(y + k) % N, span], recv_q.at[k, span], on_y(k))))
+
+    for j in range(READY):
+        product(j)
     pl.semaphore_wait(barrier, len(greeted))
+    for j in range(READY):
+        give(j)
 
     for copy in later_w:
         copy.wait()
     wall_q[pl.ds(c, 1), pl.ds(y, 1), pl.ds(z, 1)] = encode(wq[...])[None, None, None]
     wall_v[pl.ds(c, 1), pl.ds(z, 1), pl.ds(y, 1)] = encode(wv[...])[None, None, None]
-    d2d.append(send(d2d_send.at[0], d2d_recv.at[0], partner))
     w1 = []
     for k in ORDER:
         w1.append(send(wall_q.at[c, y, z], wall_q.at[c, y, z], on_z(k)))
         w1.append(send(wall_v.at[c, z, y], wall_v.at[c, z, y], on_y(k)))
-    for j in range(1, N):
+    for j in range(READY, N):
         product(j)
-        d2d.append(send(d2d_send.at[j], d2d_recv.at[j], partner))
-        combine(j - 1)
-    combine(N - 1)
-    rs1_q = [(k, send(send_q.at[(y + k) % N], recv_q.at[k], on_y(k))) for k in ORDER]
+        combine(j - READY)
+    for j in range(N - READY, N):
+        combine(j)
 
     forwards = []
 
@@ -194,19 +203,20 @@
         total_v = total_v + recv_v[k].astype(F32)
     send2_v[...] = total_v.astype(BF)
     rs2_v = [(k, send(send2_v.at[(y + k) % N], recv2_v.at[k], on_y(k))) for k in ORDER]
+    for _, _, copy in rs1_q:
+        copy.wait_recv()
     total_q = send_q[pl.ds(y, 1)][0].astype(F32)
-    for k, copy in rs1_q:
-        copy.wait_recv()
+    for k in ORDER:
         total_q = total_q + recv_q[k].astype(F32)
     send2_q[...] = total_q.astype(BF)
-    rs2_q = [(k, send(send2_q.at[(z + k) % N], recv2_q.at[k], on_z(k))) for k in ORDER]
+    rs2_q = [(k, send(send2_q.at[order.index(k)], recv2_q.at[k], on_z(k))) for k in ORDER]
     w_step(1)
 
     reduced_v = send2_v[pl.ds(y, 1)][0].astype(F32)
     for k, copy in rs2_v:
         copy.wait_recv()
         reduced_v = reduced_v + recv2_v[k].astype(F32)
-    reduced_q = send2_q[pl.ds(z, 1)][0].astype(F32)
+    reduced_q = send2_q[N - 1].astype(F32)
     for k, copy in rs2_q:
         copy.wait_recv()
         reduced_q = reduced_q + recv2_q[k].astype(F32)
@@ -269,7 +279,6 @@
 ):
     entries = D * HEADS * RK
     sums = jnp.sum(ss[...], axis=0)
-    turn = (((1,), (1,)), ((), ()))
     for which, (d, wall, b, w, f, s, step, new, copy, moment, square) in enumerate((
         (dq, wall_q, bq, wq, fq, sq, step_q, new_q, copy_q, moment_q, square_q),
         (dv, wall_v, bv, wv, fv, sv, step_v, new_v, copy_v, moment_v, square_v),
@@ -282,8 +291,8 @@
         square[...] = sqr
         high = direction.astype(BF)
         low = (direction - high.astype(F32)).astype(BF)
-        own = lax.dot_general(high, factor, turn, preferred_element_type=F32)
-        own = scale * (own + lax.dot_general(low, factor, turn, preferred_element_type=F32))
+        own = jnp.dot(high, factor, preferred_element_type=F32)
+        own = scale * (own + jnp.dot(low, factor, preferred_element_type=F32))
         step[...] = own
         new[...] = w[...] - 0.1 * own
         for z in range(N):
@@ -293,13 +302,14 @@
                 rows, codes = d[:, z], wall[:, z]
             rows = jnp.stack([rows[0], rows[1]], axis=1).reshape(2 * N * 16, 128)
             codes = jnp.stack([codes[0], codes[1]], axis=1).reshape(2 * N * 16, 256)
-            there = lax.dot_general(rows, factor, turn, preferred_element_type=F32)
+            there = jnp.dot(rows, factor, preferred_element_type=F32)
             copy[z * 256:(z + 1) * 256, :] = (decode(codes) - 0.1 * (scale * there)).astype(BF)
 
 
 def per_device(x, qc, vc, wq, wv, bq, bv, fq, sq, fv, sv):
     tokens = x.shape[0]
-    n_load, n_send = 32, 180
+    n_load, n_send = 32, 190
+    bq, bv = bq.T, bv.T
     vmem = pltpu.VMEM
     small_shape = jax.ShapeDtypeStruct
     dq, dv, wall_q, wall_v, red, ss = pl.pallas_call(
@@ -313,9 +323,9 @@
         out_specs=[ANY] * 6,
         scratch_shapes=[
             vmem((N, tokens, 256), BF), vmem((tokens, 256), BF), vmem((tokens, 256), BF),
-            vmem((256, RK), BF), vmem((256, RK), BF), vmem((16, 256), F32), vmem((16, 256), F32),
-            vmem((4, 16, 128), F32), vmem((tokens, 256), BF),
-            vmem((N, 2, N, 16, 128), F32), vmem((N, 2, N, 16, 128), BF), vmem((N, 2, N, 16, 128), BF),
+            vmem((RK, 256), BF), vmem((RK, 256), BF), vmem((16, 256), F32), vmem((16, 256), F32),
+            vmem((4, 16, 128), F32), vmem((256, tokens), BF),
+            vmem((N, 2, 2, N, 16, 128), BF), vmem((N, 2, N, 16, 128), BF),
             vmem((N, N, 16, 128), BF), vmem((N, N, 16, 128), BF),
             vmem((N, N, 16, 128), BF), vmem((N, N, 16, 128), BF),
             vmem((N, 16, 128), BF), vmem((N, 16, 128), BF), vmem((N, 16, 128), BF), vmem((N, 16, 128), BF),

time: 62.3 us -> 56.3 us (0.904)
  Pallas kernels: 58.5 us -> 55.4 us
  local copies, waits for them, and re-layouts: 2.9 us -> 0 us
    pallas_call x1, Pallas kernels: 53.6 us -> 50.6 us  [per_device(): pl.pallas_call(talk, out_shape=(small_shape((2, N, N, 16, 128), BF), smal...]
    unnamed x2 -> x0, local copies, waits for them, and re-layouts: 2.9 us -> none
where the time goes in v2:
time: 56.3 us; the launch traced here: 56.1 us
  Pallas kernels  55.4 us (98%)
  between operations  0.65 us (1%)
    pallas_call x1, Pallas kernels, per_device(): pl.pallas_call(talk, out_shape=(small_shape((2, N, N, 16, 128), BF), smal...  50.6 us
    pallas_call x1, Pallas kernels, per_device(): pl.pallas_call(finish, out_shape=(wide, wide, wide, wide, whole, whole, n...  4.85 us

profile of v2, /device:TPU:1, one launch (start us, length us, event | category | flops | bytes accessed | tf_op | source)
XLA Modules:
  0.0 56.1 jit_solution(5586400883375883247)
XLA Ops:
  0.6 50.6 %shard_map.186 = (bf16[2,8,8,16,128]{4,3,2,1,0:T(8,128)(2,1)}, bf16[2,8,8,16,128]{4,3,2,1,0:T(8,128)(2,1)}, bf16[2,8,8,16,256]{4,3,2,1,0:T(8,128)(2,1)}, bf16[2,...) custom-call(bf16[576,2048]{1,0:T(8,128)(2,1)} %x_hbm.1, bf16[576,256]{1,0:T(8,128)(2,1)} %qc_hbm.1, ...), custom_call_target="tpu_custom_call" | custom-call | tf_op jit(solution)/shard_map/pallas_call | solution.py:315
  51.2 4.9 %shard_map.187 = (f32[16,256]{1,0:T(8,128)}, f32[16,256]{1,0:T(8,128)}, f32[16,256]{1,0:T(8,128)}, f32[16,256]{1,0:T(8,128)}, bf16[2048,256]{1,0:T(8,128)(2,1)},...) custom-call(bf16[2,8,8,16,128]{4,3,2,1,0:T(8,128)(2,1)} %get-tuple-e, ...), custom_call_target="tpu_custom_call" | custom-call | tf_op jit(solution)/shard_map/pallas_call | solution.py:342
